TPU v7x, 32 devices: a whole 2x2x4 slice. The times are simulated.
32 devices in a mesh: sp: 16 (over z, y, core), tp: 2 (over x).
Axes of the slice: x: 2, y: 2, z: 4, core: 2. Of those that a mesh axis runs over, the one named last changes fastest.
Arguments:
- residual: bfloat16 [2048, 2048], P(('sp', 'tp')), may hold values from -6 to 6
- q_small: bfloat16 [2048, 1024], P('sp', 'tp'), may hold values from -6 to 6
- k_small: bfloat16 [2048, 1024], P('sp', 'tp'), may hold values from -6 to 6
- v_small: bfloat16 [2048, 1024], P('sp', 'tp'), may hold values from -6 to 6
- q_large: bfloat16 [2048, 1024], P('sp', 'tp'), may hold values from -6 to 6
- k_large: bfloat16 [2048, 1024], P('sp', 'tp'), may hold values from -6 to 6
- v_large: bfloat16 [2048, 1024], P('sp', 'tp'), may hold values from -6 to 6
- forget_small: float32 [2048, 16], P('sp', 'tp'), may hold values from 0 to 20
- forget_large: float32 [2048, 8], P('sp', 'tp'), may hold values from 0 to 20
- w_out_small: bfloat16 [1024, 2048], P('tp'), may hold values from -0.125 to 0.125
- w_out_large: bfloat16 [1024, 2048], P('tp'), may hold values from -0.125 to 0.125
- norm_gain: float32 [2048], replicated, may hold values from 0.1 to 1.9
- w_gate: bfloat16 [2048, 4096], P('sp', 'tp'), may hold values from -0.125 to 0.125
- w_up: bfloat16 [2048, 4096], P('sp', 'tp'), may hold values from -0.125 to 0.125
- conv_gate: float32 [3, 4096], P(None, 'tp'), may hold values from -3 to 3
- conv_up: float32 [3, 4096], P(None, 'tp'), may hold values from -3 to 3
- w_down: bfloat16 [4096, 2048], P('tp', 'sp'), may hold values from -0.09375 to 0.09375
Outputs:
- mixed: bfloat16 [2048, 2048], P(('sp', 'tp'))
All inputs are finite; a program needn't handle non-finite values.
Results may differ from a plain program's by a relative error of at most 0.015.
Values may be sent and summed in bfloat16 or wider, within the bound.
A program may use at most 64 MiB of HBM per device.

v0:
```python
import jax
import jax.numpy as jnp
from jax import lax
from jax.sharding import PartitionSpec as P

EPS = 1e-06
NEG = -1e30


def from_behind(block, axis, distance):
    devices = range(lax.axis_size(axis))
    route = [(i - distance, i) for i in devices if i - distance in devices]
    return lax.ppermute(block, axis, route)


def globalize(part, rows):
    heads = part.shape[1]
    blocks = part.reshape(-1, rows, heads)
    totals = blocks[:, -1, :]
    before = jnp.cumsum(totals, axis=0) - totals
    return (blocks + before[:, None, :]).reshape(part.shape)


def attend(carry, keys, values, queries, cum_own, cum_every, qpos):
    top, denom, accum = carry
    count = keys.shape[0]
    heads = queries.shape[1]
    size = queries.shape[2]
    keys = keys.reshape(count, heads, size)
    values = values.reshape(count, heads, size)
    kpos = jnp.arange(count, dtype=jnp.int32)
    scores = jnp.einsum(
        "qhd,khd->qhk", queries, keys, preferred_element_type=jnp.float32
    ) * size ** (-0.5)
    scores = scores + cum_own[:, :, None] - cum_every.T[None, :, :]
    keep = (kpos[None, :] <= qpos[:, None])[:, None, :]
    scores = jnp.where(keep, scores, NEG)
    new_top = jnp.maximum(top, jnp.max(scores, axis=-1))
    weights = jnp.where(keep, jnp.exp(scores - new_top[:, :, None]), 0.0)
    denom = jnp.sum(weights, axis=-1)
    accum = jnp.einsum(
        "qhk,khd->qhd", weights.astype(jnp.bfloat16), values, preferred_element_type=jnp.float32
    )
    return (new_top, denom, accum)


def finish(carry):
    top, denom, accum = carry
    attended = accum / denom[:, :, None]
    normed = attended * lax.rsqrt(jnp.mean(attended * attended, axis=-1, keepdims=True) + EPS)
    return normed.astype(jnp.bfloat16).reshape(attended.shape[0], -1)


def empty_carry(rows, heads, size):
    return (
        jnp.full((rows, heads), NEG, jnp.float32),
        jnp.zeros((rows, heads), jnp.float32),
        jnp.zeros((rows, heads, size), jnp.float32),
    )


def body(
    residual,
    q_small,
    k_small,
    v_small,
    q_large,
    k_large,
    v_large,
    forget_small,
    forget_large,
    w_out_small,
    w_out_large,
    norm_gain,
    w_gate,
    w_up,
    conv_gate,
    conv_up,
    w_down,
):
    rows = q_small.shape[0]
    offset = lax.axis_index("sp") * rows
    qpos = offset + jnp.arange(rows, dtype=jnp.int32)
    gathered = (
        lax.all_gather(w_gate, "sp", axis=0, tiled=True),
        lax.all_gather(w_up, "sp", axis=0, tiled=True),
        lax.all_gather(w_down, "sp", axis=1, tiled=True),
    )
    local_small = jnp.cumsum(jax.nn.log_sigmoid(forget_small), axis=0)
    local_large = jnp.cumsum(jax.nn.log_sigmoid(forget_large), axis=0)
    part_small, part_large = (
        lax.all_gather(local_small, "sp", axis=0, tiled=True),
        lax.all_gather(local_large, "sp", axis=0, tiled=True),
    )
    every_small = globalize(part_small, rows)
    every_large = globalize(part_large, rows)
    cum_small = lax.dynamic_slice_in_dim(every_small, offset, rows, 0)
    cum_large = lax.dynamic_slice_in_dim(every_large, offset, rows, 0)
    heads_small = forget_small.shape[1]
    heads_large = forget_large.shape[1]
    queries_small = q_small.reshape(rows, heads_small, -1)
    queries_large = q_large.reshape(rows, heads_large, -1)
    start_carry = (
        empty_carry(rows, heads_small, queries_small.shape[2]),
        empty_carry(rows, heads_large, queries_large.shape[2]),
    )
    keys_s = lax.all_gather(k_small, "sp", axis=0, tiled=True)
    values_s = lax.all_gather(v_small, "sp", axis=0, tiled=True)
    keys_l = lax.all_gather(k_large, "sp", axis=0, tiled=True)
    values_l = lax.all_gather(v_large, "sp", axis=0, tiled=True)
    small = attend(start_carry[0], keys_s, values_s, queries_small, cum_small, every_small, qpos)
    large = attend(start_carry[1], keys_l, values_l, queries_large, cum_large, every_large, qpos)
    normed_small = finish(small)
    normed_large = finish(large)
    first_part = jnp.dot(normed_small, w_out_small, preferred_element_type=jnp.float32)
    projected = lax.psum_scatter(
        (
            first_part + jnp.dot(normed_large, w_out_large, preferred_element_type=jnp.float32)
        ).astype(jnp.bfloat16),
        "tp",
        scatter_dimension=0,
        tiled=True,
    ).astype(jnp.float32)
    first = residual.astype(jnp.float32) + projected
    normal = (
        first * lax.rsqrt(jnp.mean(first * first, axis=-1, keepdims=True) + EPS) * norm_gain
    ).astype(jnp.bfloat16)
    gate_full, up_full, down_full = gathered
    piece = lax.all_gather(normal, "tp", axis=0, tiled=True)
    gate_part = jnp.dot(piece, gate_full, preferred_element_type=jnp.float32).astype(jnp.bfloat16)
    up_part = jnp.dot(piece, up_full, preferred_element_type=jnp.float32).astype(jnp.bfloat16)
    both = jnp.concatenate([gate_part, up_part], axis=1)
    width = both.shape[0]
    rim = from_behind(both[width - 2 :], "sp", 1)
    extended = jnp.concatenate([rim, both], axis=0).astype(jnp.float32)
    taps = jnp.concatenate([conv_gate, conv_up], axis=1)
    conv = (
        taps[0] * extended[0:width]
        + taps[1] * extended[1 : width + 1]
        + taps[2] * extended[2 : width + 2]
    )
    half = gate_full.shape[1]
    hidden = (jax.nn.silu(conv[:, :half]) * conv[:, half:]).astype(jnp.bfloat16)
    mixed = first + lax.psum_scatter(
        jnp.dot(hidden, down_full, preferred_element_type=jnp.float32).astype(jnp.bfloat16),
        "tp",
        scatter_dimension=0,
        tiled=True,
    ).astype(jnp.float32)
    return mixed.astype(jnp.bfloat16)


def solution(mesh):
    placed = (
        P(("sp", "tp"), None),
        P("sp", "tp"),
        P("sp", "tp"),
        P("sp", "tp"),
        P("sp", "tp"),
        P("sp", "tp"),
        P("sp", "tp"),
        P("sp", "tp"),
        P("sp", "tp"),
        P("tp", None),
        P("tp", None),
        P(),
        P("sp", "tp"),
        P("sp", "tp"),
        P(None, "tp"),
        P(None, "tp"),
        P("tp", "sp"),
    )
    return jax.shard_map(
        body, mesh=mesh, in_specs=placed, out_specs=P(("sp", "tp"), None), check_vma=False
    )
```

profile of v0, /device:TPU:0, one launch (start us, length us, event | category | flops | bytes accessed | tf_op | source)
XLA Modules:
  0.0 472.0 jit_solution(16428870450614130786)
XLA Ops:
  6.5 0.7 all-gather.14.cloned.1.call-update
  7.3 0.0 all-gather.8.cloned.1.call-start
  7.3 0.7 all-gather.8.cloned.1.call-update
  8.0 0.0 all-gather.12.cloned.1.call-start
  8.1 1.7 copy.44
  9.7 0.0 all-gather.10.cloned.1.call-start
  9.8 0.5 all-gather.10.cloned.1.call-update
  10.3 0.0 reduce-scatter.3.cloned.1.call-start
  10.4 0.7 fusion.40
  11.1 0.1 copy.47
  11.2 0.2 reduce_window_sum.46
  11.4 27.1 %all_gather.34 = f32[2048,4]{1,0:T(8,128)S(1)} all-gather(f32[128,4]{1,0:T(8,128)S(1)} %reduce_window_sum.46), channel_id=1, replica_groups=mesh['sp'=16,'tp'=2] {'sp'}, dimensions={0}, use_global_device_ids=true | all-gather | bytes 34816 | tf_op jit(solution)/shard_map/all_gather | solution.py:93
  38.5 0.1 bitcast_add_fusion.2
  38.6 0.1 copy.37
  38.7 0.2 reduce_window_sum.44
  38.8 24.5 %all_gather.31 = f32[2048,8]{1,0:T(8,128)S(1)} all-gather(f32[128,8]{1,0:T(8,128)S(1)} %reduce_window_sum.44), channel_id=1, replica_groups=mesh['sp'=16,'tp'=2] {'sp'}, dimensions={0}, use_global_device_ids=true | all-gather | bytes 69632 | tf_op jit(solution)/shard_map/all_gather | solution.py:92
  63.4 1.1 bitcast_add_fusion.3
  64.4 0.8 constant_dynamic-slice_fusion.1
  65.3 0.1 copy.50
  65.4 0.3 copy.51
  65.7 0.1 copy.40
  65.7 1.6 copy.41
  67.3 0.1 copy.36
  67.4 0.2 iota_compare_fusion
  67.7 4.0 copy.52
  71.7 31.4 %all-gather.8.cloned.1.call-done = bf16[2048,512]{1,0:T(8,128)(2,1)} async-done(((bf16[128,512]{1,0:T(8,128)(2,1)}), bf16[2048,512]{1,0:T(8,128)(2,1)}) %all-gather.8.cloned.1.call-update) | async-done | bytes 2097168 | tf_op jit(solution)/shard_map/all_gather | solution.py:107
  103.0 4.0 copy.35
  107.0 38.0 %all-gather.12.cloned.1.call-done = bf16[2048,512]{0,1:T(8,128)(2,1)} async-done(((bf16[128,512]{0,1:T(8,128)(2,1)}), bf16[2048,512]{0,1:T(8,128)(2,1)}) %all-gather.12.cloned.1.call-update) | async-done | bytes 2097168 | tf_op jit(solution)/shard_map/all_gather | solution.py:109
  145.0 3.7 fusion.47
  148.7 0.8 fusion.10
  149.5 0.8 copy-done.7
  150.3 1.2 multiply_reduce_fusion.1
  151.4 0.4 copy-done.6
  151.9 3.4 fusion.4
  155.3 3.2 copy-done.2
  158.5 3.1 fusion.2
  161.6 26.0 %all-gather.10.cloned.1.call-done = bf16[2048,512]{1,0:T(8,128)(2,1)} async-done(((bf16[128,512]{1,0:T(8,128)(2,1)}), bf16[2048,512]{1,0:T(8,128)(2,1)}) %all-gather.10.cloned.1.call-update) | async-done | bytes 2097168 | tf_op jit(solution)/shard_map/all_gather | solution.py:108
  187.6 3.9 copy.42
  191.5 6.6 %multiply_reduce_fusion.2 = (f32[128,8]{0,1:T(8,128)S(1)}, f32[128,8,64]{0,2,1:T(8,128)S(1)}) fusion(f32[128,8]{0,1:T(8,128)S(1)} %fusion.2, bf16[2048,8,64]{0,2,1:T(8,128)(2,1)} %bitcast.82, f32[8,2048,128]{2,1,0:T(8,128)} %copy-done.2, f32[128,8]{0,1:T(8,128)S(1)} %broadcast_maximum_fusion, f32[8,2048]{1,0:T(8,128)S(1)} %copy.41, f32[128,8]{0,1:T(8,128)S(1)} %copy.40, ...), kind=kOutput, calls=%fused_computation.49 | convolution fusion | flops 283311104 | bytes 11091968 | tf_op jit(solution)/shard_map/qhk,khd->qhd/dot_general | solution.py:41
  198.3 0.5 fusion.48
  198.8 1.0 copy-done.5
  199.7 1.3 fusion.12
  201.1 0.0 all-gather.18.cloned.1.call-start
  201.1 0.5 all-gather.18.cloned.1.call-update
  201.6 0.0 all-gather.16.cloned.1.call-start
  201.7 0.7 all-gather.16.cloned.1.call-update
  202.4 0.7 all-gather.20.cloned.1.call-update
  203.1 0.0 reduce-scatter.5.cloned.1.call-start
  203.2 11.3 %reduce-scatter.3.cloned.1.call-done = bf16[64,2048]{1,0:T(8,128)(2,1)} async-done(((bf16[128,2048]{1,0:T(8,128)(2,1)}), bf16[64,2048]{1,0:T(8,128)(2,1)}) %reduce-scatter.3.cloned.1.call-update) | async-done | bytes 262160 | tf_op jit(solution)/shard_map/reduce_scatter | solution.py:116
  214.6 1.1 multiply_reduce_fusion
  215.7 1.1 multiply_convert_fusion
  216.8 8.7 %all_gather.36 = bf16[128,2048]{1,0:T(8,128)(2,1)S(1)} all-gather(bf16[64,2048]{1,0:T(8,128)(2,1)S(1)} %multiply_convert_fusion), channel_id=1, replica_groups=mesh['sp'=16,'tp'=2] {'tp'}, dimensions={0}, use_global_device_ids=true | all-gather | bytes 786432 | tf_op jit(solution)/shard_map/all_gather | solution.py:129
  225.5 65.4 %all-gather.18.cloned.1.call-done = bf16[2048,2048]{1,0:T(8,128)(2,1)} async-done(((bf16[128,2048]{1,0:T(8,128)(2,1)}), bf16[2048,2048]{1,0:T(8,128)(2,1)}) %all-gather.18.cloned.1.call-update) | async-done | bytes 8388624 | tf_op jit(solution)/shard_map/all_gather | solution.py:86
  290.9 4.6 convolution_convert_fusion.1
  295.6 70.4 %all-gather.16.cloned.1.call-done = bf16[2048,2048]{1,0:T(8,128)(2,1)} async-done(((bf16[128,2048]{1,0:T(8,128)(2,1)}), bf16[2048,2048]{1,0:T(8,128)(2,1)}) %all-gather.16.cloned.1.call-update) | async-done | bytes 8388624 | tf_op jit(solution)/shard_map/all_gather | solution.py:85
  366.0 4.6 convolution_convert_fusion.2
  370.7 2.2 collective-permute-start
  372.9 0.8 collective-permute-done
  373.6 0.3 maximum_convert_fusion
  373.9 2.0 fusion.15
  375.9 68.5 %all-gather.20.cloned.1.call-done = bf16[2048,2048]{1,0:T(8,128)(2,1)} async-done(((bf16[2048,128]{1,0:T(8,128)(2,1)}), bf16[2048,2048]{1,0:T(8,128)(2,1)}) %all-gather.20.cloned.1.call-update) | async-done | bytes 8388624 | tf_op jit(solution)/shard_map/all_gather | solution.py:87
  444.5 6.3 %convolution_convert_fusion = bf16[128,2048]{1,0:T(8,128)(2,1)} fusion(bf16[2048,2048]{1,0:T(8,128)(2,1)} %all-gather.20.cloned.1.call-done, f32[128,4096]{1,0:T(8,128)} %fusion.15), kind=kOutput, calls=%fused_computation.16 | convolution fusion | flops 1075576832 | bytes 11010048 | tf_op jit(solution)/shard_map/dot_general | solution.py:145
  450.8 13.0 %reduce-scatter.5.cloned.1.call-done = bf16[64,2048]{1,0:T(8,128)(2,1)} async-done(((bf16[128,2048]{1,0:T(8,128)(2,1)}), bf16[64,2048]{1,0:T(8,128)(2,1)}) %reduce-scatter.5.cloned.1.call-update) | async-done | bytes 262160 | tf_op jit(solution)/shard_map/reduce_scatter | solution.py:144
  463.8 1.7 add_convert_fusion
  (46 shorter events, 0.4 us)
Async XLA Ops:
  6.5 191.7 %copy-start = (bf16[512,2048]{1,0:T(8,128)(2,1)S(1)}, bf16[512,2048]{1,0:T(8,128)(2,1)}, u32[]{:S(2)}) copy-start(bf16[512,2048]{1,0:T(8,128)(2,1)} %param.26) | copy-start | bytes 6291460
  6.5 32.0 %copy-start.12 = (f32[128,8]{0,1:T(8,128)S(1)}, f32[128,8]{0,1:T(8,128)}, u32[]{:S(2)}) copy-start(f32[128,8]{0,1:T(8,128)} %param.24) | copy-start | bytes 12292
  6.5 61.1 %all-gather.14.cloned.1.call-start = ((), (), s32[]{:S(2)}) async-start(), calls=%async_computation.5 | async-start | bytes 2228224 | tf_op jit(solution)/shard_map/all_gather | solution.py:110
  7.3 95.8 %all-gather.8.cloned.1.call-start = ((), (), s32[]{:S(2)}) async-start(), calls=%async_computation.2 | async-start | bytes 2228224 | tf_op jit(solution)/shard_map/all_gather | solution.py:107
  8.0 137.0 %all-gather.12.cloned.1.call-start = ((), (), s32[]{:S(2)}) async-start(), calls=%async_computation.4 | async-start | bytes 2228224 | tf_op jit(solution)/shard_map/all_gather | solution.py:109
  9.7 177.8 %all-gather.10.cloned.1.call-start = ((), (), s32[]{:S(2)}) async-start(), calls=%async_computation.3 | async-start | bytes 2228224 | tf_op jit(solution)/shard_map/all_gather | solution.py:108
  10.3 204.2 %reduce-scatter.3.cloned.1.call-start = ((), (), s32[]{:S(2)}) async-start(), calls=%async_computation.6 | async-start | bytes 786432 | tf_op jit(solution)/shard_map/reduce_scatter | solution.py:116
  38.4 28.9 %copy-start.8 = (bf16[128,512]{1,0:T(8,128)(2,1)S(1)}, bf16[128,512]{1,0:T(8,128)(2,1)}, u32[]{:S(2)}) copy-start(bf16[128,512]{1,0:T(8,128)(2,1)} %param.18) | copy-start | bytes 393220
  67.6 77.4 %copy-start.13 = (bf16[128,512]{1,0:T(8,128)(2,1)S(1)}, bf16[128,512]{1,0:T(8,128)(2,1)}, u32[]{:S(2)}) copy-start(bf16[128,512]{1,0:T(8,128)(2,1)} %param.21) | copy-start | bytes 393220
  148.7 1.6 copy-start.7
  150.3 1.6 copy-start.6
  155.2 3.2 copy-start.2
  198.1 1.6 copy-start.5
  198.2 5.0 %copy-start.9 = (f32[3,2048]{1,0:T(4,128)S(1)}, f32[3,2048]{1,0:T(4,128)}, u32[]{:S(2)}) copy-start(f32[3,2048]{1,0:T(4,128)} %param.31) | copy-start | bytes 73732
  198.2 5.0 %copy-start.10 = (f32[3,2048]{1,0:T(4,128)S(1)}, f32[3,2048]{1,0:T(4,128)}, u32[]{:S(2)}) copy-start(f32[3,2048]{1,0:T(4,128)} %param.32) | copy-start | bytes 73732
  198.3 16.3 %copy-start.3 = (bf16[64,2048]{1,0:T(8,128)(2,1)S(1)}, bf16[64,2048]{1,0:T(8,128)(2,1)}, u32[]{:S(2)}) copy-start(bf16[64,2048]{1,0:T(8,128)(2,1)} %param.17) | copy-start | bytes 786436
  198.3 17.5 %copy-start.11 = (f32[2048]{0:T(1024)S(1)}, f32[2048]{0:T(1024)}, u32[]{:S(2)}) copy-start(f32[2048]{0:T(1024)} %param.28) | copy-start | bytes 24580
  201.1 89.8 %all-gather.18.cloned.1.call-start = ((), (), s32[]{:S(2)}) async-start(), calls=%async_computation.8 | async-start | bytes 8912896 | tf_op jit(solution)/shard_map/all_gather | solution.py:86
  201.6 164.3 %all-gather.16.cloned.1.call-start = ((), (), s32[]{:S(2)}) async-start(), calls=%async_computation.7 | async-start | bytes 8912896 | tf_op jit(solution)/shard_map/all_gather | solution.py:85
  202.4 242.1 %all-gather.20.cloned.1.call-start = ((), (), s32[]{:S(2)}) async-start(), calls=%async_computation.9 | async-start | bytes 8912896 | tf_op jit(solution)/shard_map/all_gather | solution.py:87
  203.1 260.6 %reduce-scatter.5.cloned.1.call-start = ((), (), s32[]{:S(2)}) async-start(), calls=%async_computation.10 | async-start | bytes 786432 | tf_op jit(solution)/shard_map/reduce_scatter | solution.py:144
  370.7 3.0 collective-permute-start
  375.9 87.8 %copy-start.4 = (bf16[64,2048]{1,0:T(8,128)(2,1)S(1)}, bf16[64,2048]{1,0:T(8,128)(2,1)}, u32[]{:S(2)}) copy-start(bf16[64,2048]{1,0:T(8,128)(2,1)} %reduce-scatter.3.cloned.1.call-done) | copy-start | bytes 786436
  444.5 21.0 %copy-start.1 = (bf16[512,2048]{1,0:T(8,128)(2,1)S(1)}, bf16[512,2048]{1,0:T(8,128)(2,1)}, u32[]{:S(2)}) copy-start(bf16[512,2048]{1,0:T(8,128)(2,1)} %param.26) | copy-start | bytes 6291460
Sparse Core Ops, SparseCore 0:
  9.5 49.7 all-gather.13
  61.4 41.5 all-gather.7
  105.2 39.7 all-gather.11
  147.0 40.5 all-gather.9
  201.2 13.3 reduce-scatter.2
  216.6 74.2 all-gather.17
  293.1 72.8 all-gather.15
  368.1 76.2 all-gather.19
  450.9 12.7 reduce-scatter.4
where the time goes:
time: 473 us; the launch traced here: 472 us
  waiting for transfers between devices  329 us (70%)
  blocking collectives  60.3 us (13%)
  matrix products  32.2 us (7%)
  local copies, waits for them, and re-layouts  22.4 us (5%)
  between operations  13.5 us (3%)
  other arithmetic  12.6 us (3%)
    all_gather x1, waiting for transfers between devices, body(): lax.all_gather(w_gate, 'sp', axis=0, tiled=True)  70.4 us
    all_gather x1, waiting for transfers between devices, body(): lax.all_gather(w_down, 'sp', axis=1, tiled=True)  68.5 us
    all_gather x1, waiting for transfers between devices, body(): lax.all_gather(w_up, 'sp', axis=0, tiled=True)  65.4 us
    all_gather x1, waiting for transfers between devices, body(): keys_l = lax.all_gather(k_large, 'sp', axis=0, tiled=True)  38 us
    all_gather x1, waiting for transfers between devices, body(): keys_s = lax.all_gather(k_small, 'sp', axis=0, tiled=True)  31.4 us
    all_gather x1, blocking collectives, body(): lax.all_gather(local_large, 'sp', axis=0, tiled=True)  27.1 us
    all_gather x1, waiting for transfers between devices, body(): values_s = lax.all_gather(v_small, 'sp', axis=0, tiled=True)  26 us
    all_gather x1, blocking collectives, body(): lax.all_gather(local_small, 'sp', axis=0, tiled=True)  24.5 us
  transfers between devices with their start and end apart: 10, of which 9 were waited for; matrix products, arithmetic and copies ran while one was open for 9% of the time, Pallas kernels for 0%

commit v1 on v0

--- a/solution.py
+++ b/solution.py
@@ -1,6 +1,10 @@
+import functools
+
 import jax
 import jax.numpy as jnp
 from jax import lax
+from jax.experimental import pallas as pl
+from jax.experimental.pallas import tpu as pltpu
 from jax.sharding import PartitionSpec as P
 
 EPS = 1e-06
@@ -11,6 +15,158 @@
     devices = range(lax.axis_size(axis))
     route = [(i - distance, i) for i in devices if i - distance in devices]
     return lax.ppermute(block, axis, route)
+
+
+PLANE = 4
+
+
+def gather_kernel(n, count, *refs):
+    ins, outs = refs[:count], refs[count : 2 * count]
+    local_sem, send_sem, recv_sem = refs[2 * count :]
+    ring = n // PLANE
+    reach = (ring - 1) // 2
+    anti = ring // 2 if ring % 2 == 0 else 0
+    me = lax.axis_index("sp")
+    z, y, c = me // PLANE, lax.rem(me // 2, 2), lax.rem(me, 2)
+
+    def place(dz, flip_y, flip_c):
+        row = lax.rem(z + dz + ring, ring)
+        col = 1 - y if flip_y else y
+        core = 1 - c if flip_c else c
+        return row * PLANE + col * 2 + core
+
+    to = {"y": place(0, 1, 0), "up": place(1, 0, 0), "down": place(-1, 0, 0), "core": place(0, 0, 1)}
+
+    events = {("own",): (0, 0, None), ("y",): (0, 1, None)}
+    for other in (0, 1):
+        for k in range(1, reach + 1):
+            events[(other, "up", k)] = (-k, other, None)
+            events[(other, "down", k)] = (k, other, None)
+        if anti:
+            events[(other, "anti", 0)] = (anti, other, 0)
+            events[(other, "anti", 1)] = (anti, other, 1)
+    keys = list(events)
+    slots = {key: i for i, key in enumerate(keys)}
+    slots.update({("core", key): len(keys) + i for i, key in enumerate(keys)})
+
+    barrier = pltpu.get_barrier_semaphore()
+    for target in to.values():
+        pl.semaphore_signal(barrier, inc=1, device_id={"sp": target}, device_id_type=pl.DeviceIdType.MESH)
+    pl.semaphore_wait(barrier, len(to))
+
+    started = [[] for _ in range(count)]
+
+    def part(ref, block, half):
+        if half is None:
+            return ref.at[block]
+        rows = ref.shape[1] // 2
+        return ref.at[block, pl.ds(half * rows, rows)]
+
+    def copy_of(a, view, src, slot, target, number):
+        return pltpu.make_async_remote_copy(
+            src_ref=src,
+            dst_ref=view,
+            send_sem=send_sem.at[a, number],
+            recv_sem=recv_sem.at[a, slot],
+            device_id={"sp": target},
+            device_id_type=pl.DeviceIdType.MESH,
+        )
+
+    def send(a, key, via, as_key, half=None):
+        dz, other, own_half = events[key]
+        half = own_half if half is None else half
+        block = place(dz, other, 0)
+        view = part(outs[a], block, half)
+        src = ins[a] if key == ("own",) else view
+        copy = copy_of(a, view, src, slots[as_key], to[via], len(started[a]))
+        copy.start()
+        started[a].append(copy)
+
+    def arrived(a, key, from_core=False):
+        dz, other, half = events[key]
+        view = part(outs[a], place(dz, other, int(from_core)), half)
+        slot = slots[("core", key)] if from_core else slots[key]
+        copy_of(a, view, view, slot, to["core"], 0).wait_recv()
+
+    def onward(a, key):
+        other, way, k = key
+        arrived(a, key)
+        if way != "anti" and k < reach:
+            send(a, key, way, (other, way, k + 1))
+        elif way != "anti" and anti and not other:
+            half = 0 if way == "up" else 1
+            send(a, key, way, (other, "anti", half), half)
+        elif way == "anti" and not other:
+            send(a, key, "y", (1, "anti", k))
+        send(a, key, "core", ("core", key))
+
+    locals_ = []
+
+    def stage0(a):
+        copy = pltpu.make_async_copy(ins[a], outs[a].at[me], local_sem.at[a])
+        copy.start()
+        locals_.append(copy)
+        send(a, ("own",), "y", ("y",))
+        send(a, ("own",), "up", (0, "up", 1))
+        send(a, ("own",), "down", (0, "down", 1))
+        send(a, ("own",), "core", ("core", ("own",)))
+
+    def stage1(a):
+        arrived(a, ("y",))
+        send(a, ("y",), "up", (1, "up", 1))
+        send(a, ("y",), "down", (1, "down", 1))
+        send(a, ("y",), "core", ("core", ("y",)))
+        for k in range(1, reach + 1):
+            onward(a, (0, "up", k))
+            onward(a, (0, "down", k))
+
+    def stage2(a):
+        if anti:
+            onward(a, (0, "anti", 0))
+            onward(a, (0, "anti", 1))
+        for k in range(1, reach + 1):
+            onward(a, (1, "up", k))
+            onward(a, (1, "down", k))
+
+    def stage3(a):
+        if anti:
+            onward(a, (1, "anti", 0))
+            onward(a, (1, "anti", 1))
+
+    def stage4(a):
+        for key in keys:
+            arrived(a, key, from_core=True)
+
+    stage0(0)
+    for tick in range(1, count + 6):
+        for lag, stage in enumerate((stage0, None, stage1, stage2, stage3, stage4)):
+            a = tick - lag
+            if stage is not None and 0 <= a < count and not (stage is stage0 and a == 0):
+                stage(a)
+    for a in range(count):
+        locals_[a].wait()
+        for copy in started[a]:
+            copy.wait_send()
+
+
+def gather_all(arrays):
+    n = lax.axis_size("sp")
+    ring = n // PLANE
+    if n % PLANE or ring < 3:
+        return [lax.all_gather(x, "sp", axis=0) for x in arrays]
+    count = len(arrays)
+    return pl.pallas_call(
+        functools.partial(gather_kernel, n, count),
+        out_shape=[jax.ShapeDtypeStruct((n,) + x.shape, x.dtype) for x in arrays],
+        in_specs=[pl.BlockSpec(memory_space=pltpu.VMEM)] * count,
+        out_specs=[pl.BlockSpec(memory_space=pl.ANY)] * count,
+        scratch_shapes=[
+            pltpu.SemaphoreType.DMA((count,)),
+            pltpu.SemaphoreType.DMA((count, n // 2 * 3)),
+            pltpu.SemaphoreType.DMA((count, n + 8)),
+        ],
+        compiler_params=pltpu.CompilerParams(collective_id=0, has_side_effects=True),
+    )(*arrays)
 
 
 def globalize(part, rows):
@@ -81,33 +237,29 @@
     rows = q_small.shape[0]
     offset = lax.axis_index("sp") * rows
     qpos = offset + jnp.arange(rows, dtype=jnp.int32)
-    gathered = (
-        lax.all_gather(w_gate, "sp", axis=0, tiled=True),
-        lax.all_gather(w_up, "sp", axis=0, tiled=True),
-        lax.all_gather(w_down, "sp", axis=1, tiled=True),
-    )
     local_small = jnp.cumsum(jax.nn.log_sigmoid(forget_small), axis=0)
     local_large = jnp.cumsum(jax.nn.log_sigmoid(forget_large), axis=0)
-    part_small, part_large = (
-        lax.all_gather(local_small, "sp", axis=0, tiled=True),
-        lax.all_gather(local_large, "sp", axis=0, tiled=True),
-    )
-    every_small = globalize(part_small, rows)
-    every_large = globalize(part_large, rows)
+    heads_small = forget_small.shape[1]
+    heads_large = forget_large.shape[1]
+    local = jnp.concatenate([local_small, local_large], axis=1).T
+    padded = jnp.pad(local, ((0, -local.shape[0] % 16), (0, 0)))
+    every, keys_s, values_s, keys_l, values_l, gate_full, up_full, down_blocks = gather_all(
+        [padded, k_small, v_small, k_large, v_large, w_gate, w_up, w_down]
+    )
+    flat = lambda x: x.reshape(-1, x.shape[-1])
+    keys_s, values_s, keys_l, values_l = map(flat, (keys_s, values_s, keys_l, values_l))
+    gate_full, up_full = flat(gate_full), flat(up_full)
+    part = every.transpose(0, 2, 1).reshape(-1, padded.shape[0])
+    every_small = globalize(part[:, :heads_small], rows)
+    every_large = globalize(part[:, heads_small : heads_small + heads_large], rows)
     cum_small = lax.dynamic_slice_in_dim(every_small, offset, rows, 0)
     cum_large = lax.dynamic_slice_in_dim(every_large, offset, rows, 0)
-    heads_small = forget_small.shape[1]
-    heads_large = forget_large.shape[1]
     queries_small = q_small.reshape(rows, heads_small, -1)
     queries_large = q_large.reshape(rows, heads_large, -1)
     start_carry = (
         empty_carry(rows, heads_small, queries_small.shape[2]),
         empty_carry(rows, heads_large, queries_large.shape[2]),
     )
-    keys_s = lax.all_gather(k_small, "sp", axis=0, tiled=True)
-    values_s = lax.all_gather(v_small, "sp", axis=0, tiled=True)
-    keys_l = lax.all_gather(k_large, "sp", axis=0, tiled=True)
-    values_l = lax.all_gather(v_large, "sp", axis=0, tiled=True)
     small = attend(start_carry[0], keys_s, values_s, queries_small, cum_small, every_small, qpos)
     large = attend(start_carry[1], keys_l, values_l, queries_large, cum_large, every_large, qpos)
     normed_small = finish(small)
@@ -125,7 +277,6 @@
     normal = (
         first * lax.rsqrt(jnp.mean(first * first, axis=-1, keepdims=True) + EPS) * norm_gain
     ).astype(jnp.bfloat16)
-    gate_full, up_full, down_full = gathered
     piece = lax.all_gather(normal, "tp", axis=0, tiled=True)
     gate_part = jnp.dot(piece, gate_full, preferred_element_type=jnp.float32).astype(jnp.bfloat16)
     up_part = jnp.dot(piece, up_full, preferred_element_type=jnp.float32).astype(jnp.bfloat16)
@@ -142,7 +293,9 @@
     half = gate_full.shape[1]
     hidden = (jax.nn.silu(conv[:, :half]) * conv[:, half:]).astype(jnp.bfloat16)
     mixed = first + lax.psum_scatter(
-        jnp.dot(hidden, down_full, preferred_element_type=jnp.float32).astype(jnp.bfloat16),
+        jnp.einsum("th,nhc->tnc", hidden, down_blocks, preferred_element_type=jnp.float32)
+        .astype(jnp.bfloat16)
+        .reshape(width, -1),
         "tp",
         scatter_dimension=0,
         tiled=True,

time: 473 us -> 395 us (0.84)
  waiting for transfers between devices: 329 us -> 29.7 us
  Pallas kernels: 0 us -> 247 us
  blocking collectives: 60.3 us -> 8.9 us
  local copies, waits for them, and re-layouts: 22.4 us -> 46 us
  other arithmetic: 12.6 us -> 18 us
    all_gather x7 -> x0, waiting for transfers between devices: 300 us -> none  [the longest x1 70.4 us: body(): lax.all_gather(w_gate, 'sp', axis=0, tiled=True)]
    pallas_call x0 -> x1, Pallas kernels: none -> 247 us  [gather_all(): pl.pallas_call(functools.partial(gather_kernel, n, count), out_shape=[jax...]
    all_gather x2 -> x0, blocking collectives: 51.6 us -> none  [the longest x1 27.1 us: body(): lax.all_gather(local_large, 'sp', axis=0, tiled=True)]
    pallas_call x0 -> x3, local copies, waits for them, and re-layouts: none -> 21.5 us  [gather_all(): pl.pallas_call(functools.partial(gather_kernel, n, count), out_shape=[jax...]
    another operation x0 -> x6, local copies, waits for them, and re-layouts: none -> 16.6 us  [the longest x2 8.37 us: attend(): keys = keys.reshape(count, heads, size)]
    all_gather x3 -> x0, local copies, waits for them, and re-layouts: 12 us -> none  [the longest x1 4.02 us: body(): values_l = lax.all_gather(v_large, 'sp', axis=0, tiled=True)]
    dot_general x1 -> x0, matrix products: 6.31 us -> none  [body(): jnp.dot(hidden, down_full, preferred_element_type=jnp.float32)]
    reduce_sum x2, other arithmetic: 3.85 us -> 9.73 us  [attend(): denom = jnp.sum(weights, axis=-1)]
  transfers between devices with their start and end apart: 10 -> 3, of which waited for: 9 -> 2; matrix products, arithmetic and copies ran while one was open for 9% -> 3% of each run, Pallas kernels for 0% -> 0%
where the time goes in v1:
time: 395 us; the launch traced here: 394 us
  Pallas kernels  247 us (63%)
  local copies, waits for them, and re-layouts  46 us (12%)
  waiting for transfers between devices  29.7 us (8%)
  matrix products  29.5 us (7%)
  other arithmetic  18 us (5%)
  between operations  13.8 us (3%)
  blocking collectives  8.9 us (2%)
    pallas_call x1, Pallas kernels, gather_all(): pl.pallas_call(functools.partial(gather_kernel, n, count), out_shape=[jax...  247 us
    pallas_call x3, local copies, waits for them, and re-layouts, gather_all(): pl.pallas_call(functools.partial(gather_kernel, n, count), out_shape=[jax...  21.5 us
    reduce_scatter x1, waiting for transfers between devices, body(): lax.psum_scatter(jnp.einsum('th,nhc->tnc', hidden, down_blocks, preferred...  15.7 us
    reduce_scatter x1, waiting for transfers between devices, body(): lax.psum_scatter((first_part + jnp.dot(normed_large, w_out_large, preferr...  13.9 us
    dot_general x2, matrix products, attend(): jnp.einsum('qhd,khd->qhk', queries, keys, preferred_element_type=jnp.floa...  10.8 us
    reduce_sum x2, other arithmetic, attend(): denom = jnp.sum(weights, axis=-1)  9.73 us
    all_gather x1, blocking collectives, body(): piece = lax.all_gather(normal, 'tp', axis=0, tiled=True)  8.9 us
    dot_general x2, matrix products, attend(): jnp.einsum('qhk,khd->qhd', weights.astype(jnp.bfloat16), values, preferre...  8.45 us
  transfers between devices with their start and end apart: 3, of which 2 were waited for; matrix products, arithmetic and copies ran while one was open for 3% of the time, Pallas kernels for 0%

profile of v1, /device:TPU:0, one launch (start us, length us, event | category | flops | bytes accessed | tf_op | source)
XLA Modules:
  0.0 394.2 jit_solution(9031642231006580109)
XLA Ops:
  6.5 0.0 copy-start
  6.5 0.8 fusion.46
  7.4 0.1 copy.37
  7.5 0.2 reduce_window_sum.44
  7.7 0.7 fusion.47
  8.4 0.1 copy.38
  8.6 0.2 reduce_window_sum.45
  8.7 0.1 copy.40
  8.8 0.6 pad.4.refs_0_
  9.4 246.9 %shard_map.163 = (f32[16,16,128]{2,1,0:T(8,128)}, bf16[16,128,512]{2,1,0:T(8,128)(2,1)}, bf16[16,128,512]{2,1,0:T(8,128)(2,1)}, bf16[16,128,512]{2,1,0:T(8,128)(...) custom-call(f32[16,128]{1,0:T(8,128)} %pad.4.refs_0_, ...), custom_call_target="tpu_custom_call" | custom-call | tf_op jit(solution)/shard_map/pallas_call | solution.py:158
  256.4 0.9 copy_bitcast_fusion
  257.3 0.4 copy.51
  257.7 0.1 copy.52
  257.8 0.1 broadcast_bitcast_fusion
  257.9 0.2 iota_compare_fusion
  258.1 4.2 %reshape_reshape.15 = bf16[2048,4,128]{2,1,0:T(4,128)(2,1)} reshape(bf16[16,128,512]{2,1,0:T(8,128)(2,1)} %get-tuple-element.17) | data formatting | bytes 4194304 | tf_op jit(solution)/shard_map/reshape;reshape | solution.py:185
  262.3 4.1 %fusion.54 = (f32[128,4]{0,1:T(4,128)S(1)}, f32[128,4,2048]{0,2,1:T(8,128)}) fusion(f32[4,2048]{1,0:T(4,128)S(1)} %bitcast.111, f32[128,4]{0,1:T(4,128)S(1)} %constant_dynamic-slice_fusion, bf16[2048,4,128]{2,1,0:T(4,128)(2,1)} %reshape_reshape.15, pred[128,2048]{0,1:T(8,128)(4,1)S(1)} %iota_compare_fusion, bf16[128,512]{1,0:T(8,128)(2,1)S(1)} %copy-done.14), kind=kOutput, calls=%fused_computation.80 | convolution fusion | flops 273677824 | bytes 6721536 | tf_op jit(solution)/shard_map/qhd,khd->qhk/dot_general | solution.py:188
  266.4 4.0 %reshape_reshape.14 = bf16[2048,4,128]{2,1,0:T(4,128)(2,1)} reshape(bf16[16,128,512]{2,1,0:T(8,128)(2,1)} %get-tuple-element.16) | data formatting | bytes 4194304 | tf_op jit(solution)/shard_map/reshape;reshape | solution.py:186
  270.4 3.1 fusion.10
  273.5 0.3 copy-done.4
  273.8 3.6 multiply_reduce_fusion.1
  277.4 0.0 slice-done.2
  277.4 0.3 copy.45
  277.8 0.9 bitcast_add_fusion.2
  278.7 0.0 copy-start.10
  278.7 4.6 %copy.42 = bf16[16,128,512]{1,0,2:T(8,128)(2,1)} copy(bf16[16,128,512]{2,1,0:T(8,128)(2,1)} %get-tuple-element.14) | data formatting | bytes 4194304 | tf_op jit(solution)/shard_map/pallas_call | solution.py:158
  283.3 4.2 %reshape_reshape.13 = bf16[2048,8,64]{0,2,1:T(8,128)(2,1)} reshape(bf16[16,128,512]{1,0,2:T(8,128)(2,1)} %copy.42) | data formatting | bytes 4194304 | tf_op jit(solution)/shard_map/reshape;reshape | solution.py:185
  287.5 0.1 copy.43
  287.6 6.7 %fusion.4 = (f32[128,8]{0,1:T(8,128)S(1)}, f32[8,2048,128]{2,1,0:T(8,128)}) fusion(f32[8,2048]{1,0:T(8,128)S(1)} %bitcast.104, f32[128,8]{0,1:T(8,128)S(1)} %constant_dynamic-slice_fusion.1, pred[128,2048]{0,1:T(8,128)(4,1)S(1)} %iota_compare_fusion, bf16[2048,8,64]{0,2,1:T(8,128)(2,1)} %reshape_reshape.13, bf16[128,8,64]{0,2,1:T(8,128)(2,1)S(1)} %bitcast.107), kind=kOutput, calls=%fused_computation.6 | convolution fusion | flops 278920192 | bytes 10952704 | tf_op jit(solution)/shard_map/qhd,khd->qhk/dot_general | solution.py:188
  294.3 4.5 %copy.41 = bf16[16,128,512]{1,0,2:T(8,128)(2,1)} copy(bf16[16,128,512]{2,1,0:T(8,128)(2,1)} %get-tuple-element.13) | data formatting | bytes 4194304 | tf_op jit(solution)/shard_map/pallas_call | solution.py:158
  298.8 4.2 %reshape_reshape.12 = bf16[2048,8,64]{0,2,1:T(8,128)(2,1)} reshape(bf16[16,128,512]{1,0,2:T(8,128)(2,1)} %copy.41) | data formatting | bytes 4194304 | tf_op jit(solution)/shard_map/reshape;reshape | solution.py:186
  303.0 6.6 %fusion.2 = f32[128,8]{0,1:T(8,128)S(1)} fusion(f32[8,2048,128]{2,1,0:T(8,128)} %get-tuple-element.25, f32[128,8]{0,1:T(8,128)S(1)} %broadcast_maximum_fusion, f32[8,2048]{1,0:T(8,128)S(1)} %bitcast.105, f32[128,8]{0,1:T(8,128)S(1)} %constant_dynamic-slice_fusion.1, pred[128,2048]{0,1:T(8,128)(4,1)S(1)} %iota_compare_fusion), kind=kLoop, calls=%fused_computation.4 | loop fusion | flops 14679040 | bytes 8728576 | tf_op jit(solution)/shard_map/reduce_sum | solution.py:196
  309.6 0.0 copy-start.9
  309.6 4.9 %multiply_reduce_fusion.2 = (f32[128,8]{0,1:T(8,128)S(1)}, f32[128,8,64]{0,2,1:T(8,128)S(1)}) fusion(f32[128,8]{0,1:T(8,128)S(1)} %fusion.2, bf16[2048,8,64]{0,2,1:T(8,128)(2,1)} %reshape_reshape.12, f32[8,2048,128]{2,1,0:T(8,128)S(1)} %copy-done.2, f32[128,8]{0,1:T(8,128)S(1)} %broadcast_maximum_fusion, f32[8,2048]{1,0:T(8,128)S(1)} %bitcast.106, ...), kind=kOutput, calls=%fused_computation.49 | convolution fusion | flops 283311104 | bytes 11091968 | tf_op jit(solution)/shard_map/qhk,khd->qhd/dot_general | solution.py:197
  314.5 0.0 copy-start.7
  314.6 0.0 copy-done.9
  314.6 0.0 copy-start.11
  314.6 0.0 copy-start.12
  314.6 0.0 copy-start.5
  314.7 0.0 copy-start.13
  314.7 0.5 fusion.55
  315.2 1.0 copy-done.7
  316.1 1.3 fusion.12
  317.5 0.0 reduce-scatter.3.cloned.1.call-update
  317.5 0.0 reduce-scatter.5.cloned.1.call-start
  317.6 13.9 %reduce-scatter.3.cloned.1.call-done = bf16[64,2048]{1,0:T(8,128)(2,1)} async-done(((bf16[128,2048]{1,0:T(8,128)(2,1)}), bf16[64,2048]{1,0:T(8,128)(2,1)}) %reduce-scatter.3.cloned.1.call-update) | async-done | bytes 262160 | tf_op jit(solution)/shard_map/reduce_scatter | solution.py:268
  331.5 1.1 multiply_reduce_fusion
  332.7 0.0 slice-start
  332.7 1.2 multiply_convert_fusion
  333.9 8.9 %all_gather.3 = bf16[128,2048]{1,0:T(8,128)(2,1)S(1)} all-gather(bf16[64,2048]{1,0:T(8,128)(2,1)S(1)} %multiply_convert_fusion), channel_id=1, replica_groups=mesh['sp'=16,'tp'=2] {'tp'}, dimensions={0}, use_global_device_ids=true | all-gather | bytes 786432 | tf_op jit(solution)/shard_map/all_gather | solution.py:280
  342.8 4.8 %convolution_convert_fusion.1 = bf16[128,2048]{1,0:T(8,128)(2,1)S(1)} fusion(bf16[128,2048]{1,0:T(8,128)(2,1)S(1)} %all_gather.3, bf16[2048,2048]{1,0:T(8,128)(2,1)} %bitcast.96), kind=kOutput, calls=%fused_computation.17 | convolution fusion | flops 1074003968 | bytes 9437184 | tf_op jit(solution)/shard_map/dot_general | solution.py:281
  347.6 1.3 convolution_convert_fusion
  349.0 1.3 collective-permute-start
  350.3 12.4 %copy.55 = bf16[16,2048,128]{1,2,0:T(8,128)(2,1)} copy(bf16[16,2048,128]{2,1,0:T(8,128)(2,1)} %get-tuple-element.20) | data formatting | bytes 16777216 | tf_op jit(solution)/shard_map/pallas_call | solution.py:158
  362.7 0.0 collective-permute-done
  362.7 0.3 maximum_convert_fusion
  363.0 0.6 fusion.15
  363.6 2.8 copy-done.3
  366.4 2.4 fusion.39
  368.8 0.1 convert_element_type.59
  368.9 1.0 copy.60
  369.9 0.0 reduce-scatter.5.cloned.1.call-update
  369.9 15.7 %reduce-scatter.5.cloned.1.call-done = bf16[64,2048]{1,0:T(8,128)(2,1)} async-done(((bf16[128,2048]{1,0:T(8,128)(2,1)}), bf16[64,2048]{1,0:T(8,128)(2,1)}) %reduce-scatter.5.cloned.1.call-update) | async-done | bytes 262160 | tf_op jit(solution)/shard_map/reduce_scatter | solution.py:295
  385.6 1.7 add_convert_fusion
  (44 shorter events, 0.4 us)
Async XLA Ops:
  6.5 308.2 %copy-start = (bf16[512,2048]{1,0:T(8,128)(2,1)S(1)}, bf16[512,2048]{1,0:T(8,128)(2,1)}, u32[]{:S(2)}) copy-start(bf16[512,2048]{1,0:T(8,128)(2,1)} %param.26) | copy-start | bytes 6291460
  6.5 325.0 %reduce-scatter.3.cloned.1.call-start = ((), (), s32[]{:S(2)}) async-start(), calls=%async_computation.2 | async-start | bytes 786432 | tf_op jit(solution)/shard_map/reduce_scatter | solution.py:268
  8.7 253.6 %copy-start.14 = (bf16[128,512]{1,0:T(8,128)(2,1)S(1)}, bf16[128,512]{1,0:T(8,128)(2,1)}, u32[]{:S(2)}) copy-start(bf16[128,512]{1,0:T(8,128)(2,1)} %param.21) | copy-start | bytes 393220
  257.3 9.1 %copy-start.8 = (f32[2048,16]{0,1:T(8,128)}, f32[2048,16]{0,1:T(8,128)S(1)}, u32[]{:S(2)}) copy-start(f32[2048,16]{0,1:T(8,128)S(1)} %copy_bitcast_fusion) | copy-start | bytes 393220
  270.4 3.4 copy-start.4
  273.8 3.6 slice-start.2
  278.7 8.8 %copy-start.10 = (bf16[128,512]{1,0:T(8,128)(2,1)S(1)}, bf16[128,512]{1,0:T(8,128)(2,1)}, u32[]{:S(2)}) copy-start(bf16[128,512]{1,0:T(8,128)(2,1)} %param.18) | copy-start | bytes 393220
  303.0 6.6 %copy-start.2 = (f32[8,2048,128]{2,1,0:T(8,128)S(1)}, f32[8,2048,128]{2,1,0:T(8,128)}, u32[]{:S(2)}) copy-start(f32[8,2048,128]{2,1,0:T(8,128)} %get-tuple-element.25) | copy-start | bytes 25165828
  309.6 4.9 %copy-start.9 = (f32[128,4,128]{0,2,1:T(8,128)S(1)}, f32[128,4,128]{0,2,1:T(8,128)}, u32[]{:S(2)}) copy-start(f32[128,4,128]{0,2,1:T(8,128)} %get-tuple-element.31) | copy-start | bytes 786436
  314.5 1.6 copy-start.7
  314.6 3.0 copy-start.11
  314.6 3.0 copy-start.12
  314.6 16.9 %copy-start.5 = (bf16[64,2048]{1,0:T(8,128)(2,1)S(1)}, bf16[64,2048]{1,0:T(8,128)(2,1)}, u32[]{:S(2)}) copy-start(bf16[64,2048]{1,0:T(8,128)(2,1)} %param.17) | copy-start | bytes 786436
  314.7 18.0 %copy-start.13 = (f32[2048]{0:T(1024)S(1)}, f32[2048]{0:T(1024)}, u32[]{:S(2)}) copy-start(f32[2048]{0:T(1024)} %param.28) | copy-start | bytes 24580
  317.5 68.2 %reduce-scatter.5.cloned.1.call-start = ((), (), s32[]{:S(2)}) async-start(), calls=%async_computation.3 | async-start | bytes 786432 | tf_op jit(solution)/shard_map/reduce_scatter | solution.py:295
  332.7 14.9 %slice-start = ((s8[8388608]{0:T(1024)(128)(4,1)}), s8[4194304]{0:T(1024)(128)(4,1)S(1)}, s32[]{:S(2)}) async-start(s8[8388608]{0:T(1024)(128)(4,1)} %bitcast.93), calls=%async_computation.4 | async-start | bytes 8388608
  342.8 4.8 %slice-start.1 = ((s8[8388608]{0:T(1024)(128)(4,1)}), s8[4194304]{0:T(1024)(128)(4,1)S(1)}, s32[]{:S(2)}) async-start(s8[8388608]{0:T(1024)(128)(4,1)} %bitcast.93), calls=%async_computation.5 | async-start | bytes 8388608
  349.0 13.7 %collective-permute-start = (bf16[2,4096]{1,0:T(2,128)(2,1)S(1)}, bf16[2,4096]{1,0:T(2,128)(2,1)S(1)}, u32[]{:S(2)}, u32[]{:S(2)}) collective-permute-start(bf16[2,4096]{1,0:T(2,128)(2,1)S(1)} %pad_maximum_fusion), channel_id=1, source_target_pairs={{0,2},{2,4},{4,6},{6,8},{8,10},{10,12},{12,14},{14,16},{16,18},{18... | collective-permute-start | bytes 49160 | tf_op jit(solution)/shard_map/ppermute | solution.py:17
  363.0 3.4 copy-start.3
  366.4 19.3 %copy-start.6 = (bf16[64,2048]{1,0:T(8,128)(2,1)S(1)}, bf16[64,2048]{1,0:T(8,128)(2,1)}, u32[]{:S(2)}) copy-start(bf16[64,2048]{1,0:T(8,128)(2,1)} %reduce-scatter.3.cloned.1.call-done) | copy-start | bytes 786436
  366.4 21.0 %copy-start.1 = (bf16[512,2048]{1,0:T(8,128)(2,1)S(1)}, bf16[512,2048]{1,0:T(8,128)(2,1)}, u32[]{:S(2)}) copy-start(bf16[512,2048]{1,0:T(8,128)(2,1)} %param.26) | copy-start | bytes 6291460
Sparse Core Ops, SparseCore 0:
  317.6 13.8 reduce-scatter.2
  370.0 15.5 reduce-scatter.4

commit v2 on v0

v2 whole, which is shorter than its diff:
```python
import functools

import jax
import jax.numpy as jnp
from jax import lax
from jax.experimental import pallas as pl
from jax.experimental.pallas import tpu as pltpu
from jax.sharding import PartitionSpec as P

EPS = 1e-06
NEG = -1e30


def from_behind(block, axis, distance):
    devices = range(lax.axis_size(axis))
    route = [(i - distance, i) for i in devices if i - distance in devices]
    return lax.ppermute(block, axis, route)


PLANE = 4
PIECE = 1 << 18
UP, DOWN, UP_OTHER, DOWN_OTHER, ACROSS, CORE, CORE_OTHER = range(7)
OWN, OTHER = 0, 1
MESH = pl.DeviceIdType.MESH


def gather_kernel(n, count, items, *refs):
    ins, outs = refs[:count], refs[count : 2 * count]
    local_sem, send_sem, recv_sem = refs[2 * count :]
    line = n // PLANE
    me = lax.axis_index("sp")
    z, y, c = me // PLANE, lax.rem(me // 2, 2), lax.rem(me, 2)

    def place(row, flip_y, flip_c):
        return row * PLANE + (1 - y if flip_y else y) * 2 + (1 - c if flip_c else c)

    across, core = place(z, 1, 0), place(z, 0, 1)
    above, below = place(jnp.minimum(z + 1, line - 1), 0, 0), place(jnp.maximum(z - 1, 0), 0, 0)
    barrier = pltpu.get_barrier_semaphore()

    def greet(target):
        pl.semaphore_signal(barrier, inc=1, device_id={"sp": target}, device_id_type=MESH)

    greet(across)
    greet(core)
    pl.when(z < line - 1)(lambda: greet(above))
    pl.when(z > 0)(lambda: greet(below))
    pl.semaphore_wait(barrier, 2 + jnp.minimum(z, 1) + jnp.minimum(line - 1 - z, 1))

    def view(i, row, other, other_core=0):
        a, start, size, _ = items[i]
        return outs[a].at[place(row, other, other_core), pl.ds(start, size)]

    def copy_of(i, src, dst, via, row, slot, target):
        return pltpu.make_async_remote_copy(
            src_ref=src,
            dst_ref=dst,
            send_sem=send_sem.at[i, via, row],
            recv_sem=recv_sem.at[i, slot, row],
            device_id={"sp": target},
            device_id_type=MESH,
        )

    def send(i, via, row, other, first=False):
        dst = view(i, row, other)
        a, start, size, _ = items[i]
        src = ins[a].at[pl.ds(start, size)] if first else dst
        target = {UP: above, UP_OTHER: above, DOWN: below, DOWN_OTHER: below, ACROSS: across}.get(via, core)
        slot = {ACROSS: OTHER, CORE: 2 + OWN, CORE_OTHER: 2 + OTHER}.get(via, other)
        return copy_of(i, src, dst, via, row, slot, target)

    def arrived(i, row, other):
        copy_of(i, view(i, row, other), view(i, row, other), CORE, row, other, core).wait_recv()

    def on_z(i, other, k, act, kinds):
        up, down = (UP_OTHER, DOWN_OTHER) if other else (UP, DOWN)

        @pl.when(z - k >= 0)
        def _():
            if "wait" in kinds:
                arrived(i, z - k, other)
            pl.when(z < line - 1)(lambda: act(send(i, up, z - k, other)))
            onward(i, z - k, other, act)

        @pl.when(z + k <= line - 1)
        def _():
            if "wait" in kinds:
                arrived(i, z + k, other)
            pl.when(z > 0)(lambda: act(send(i, down, z + k, other)))
            onward(i, z + k, other, act)

    def onward(i, row, other, act):
        if not other and not items[i][3]:
            act(send(i, ACROSS, row, 0))
        act(send(i, CORE_OTHER if other else CORE, row, other))

    start = lambda copy: copy.start()
    finish_send = lambda copy: copy.wait_send()

    def local(i):
        a, first, size, _ = items[i]
        return pltpu.make_async_copy(ins[a].at[pl.ds(first, size)], view(i, z, 0), local_sem.at[i])

    def stage_own(i, act):
        pl.when(z < line - 1)(lambda: act(send(i, UP, z, 0, True)))
        pl.when(z > 0)(lambda: act(send(i, DOWN, z, 0, True)))
        act(send(i, ACROSS, z, 0, True))
        act(send(i, CORE, z, 0, True))

    def stage_column(i, act, kinds):
        if "wait" in kinds:
            arrived(i, z, 1)
        pl.when(z < line - 1)(lambda: act(send(i, UP_OTHER, z, 1)))
        pl.when(z > 0)(lambda: act(send(i, DOWN_OTHER, z, 1)))
        act(send(i, CORE_OTHER, z, 1))

    def stage(i, k, act, kinds):
        early = items[i][3]
        if k == 0:
            if "wait" in kinds:
                local(i).start()
            stage_own(i, act)
        elif k < line:
            on_z(i, 0, k, act, kinds)
        if early and k == 1:
            stage_column(i, act, kinds)
        if early and 2 <= k <= line:
            on_z(i, 1, k - 1, act, kinds)
        if not early and k == line:
            for row in range(line):
                if "wait" in kinds:
                    arrived(i, row, 1)
                act(send(i, CORE_OTHER, row, 1))
        if k == line + 1 and "wait" in kinds:
            for row in range(line):
                for other in (0, 1):
                    dst = view(i, row, other, 1)
                    copy_of(i, dst, dst, CORE, row, 2 + other, core).wait_recv()

    total = len(items)
    stage(0, 0, start, ("wait",))
    stage(1, 0, start, ("wait",))
    for tick in range(1, total + line + 2):
        if 1 < tick + 1 < total:
            stage(tick + 1, 0, start, ("wait",))
        for k in range(1, line + 2):
            if 0 <= tick - k < total:
                stage(tick - k, k, start, ("wait",))
    for i in range(total):
        local(i).wait()
        for k in range(line + 1):
            stage(i, k, finish_send, ())


def gather_all(arrays, early):
    n = lax.axis_size("sp")
    line = n // PLANE
    if n % PLANE or line < 2:
        return [lax.all_gather(x, "sp", axis=0) for x in arrays]
    count = len(arrays)
    items = []
    for a, x in enumerate(arrays):
        rows = x.shape[0]
        pieces = max(1, x.size * x.dtype.itemsize // PIECE)
        while rows % (16 * pieces) and pieces > 1:
            pieces -= 1
        items += [(a, j * (rows // pieces), rows // pieces, early[a]) for j in range(pieces)]
    total = len(items)
    return pl.pallas_call(
        functools.partial(gather_kernel, n, count, items),
        out_shape=[jax.ShapeDtypeStruct((n,) + x.shape, x.dtype) for x in arrays],
        in_specs=[pl.BlockSpec(memory_space=pltpu.VMEM)] * count,
        out_specs=[pl.BlockSpec(memory_space=pl.ANY)] * count,
        scratch_shapes=[
            pltpu.SemaphoreType.DMA((total,)),
            pltpu.SemaphoreType.DMA((total, 7, line)),
            pltpu.SemaphoreType.DMA((total, 4, line)),
        ],
        compiler_params=pltpu.CompilerParams(collective_id=0, has_side_effects=True),
    )(*arrays)


def attention_kernel(rows, per, size_s, size_l, cum, q_s, k_s, v_s, q_l, k_l, v_l, out_s, out_l):
    offset = pl.multiple_of(lax.axis_index("sp") * rows, rows)
    own = cum[:, pl.ds(offset, rows)].T
    keep = None

    def head(q, k_ref, v_ref, row, size):
        lanes = k_ref.shape[-1]
        keys = k_ref[...].reshape(-1, lanes)
        values = v_ref[...].reshape(-1, lanes)
        nonlocal keep
        if keep is None:
            shape = (rows, keys.shape[0])
            keep = lax.broadcasted_iota(jnp.int32, shape, 1) <= offset + lax.broadcasted_iota(
                jnp.int32, shape, 0
            )
        scores = lax.dot_general(
            q, keys, (((1,), (1,)), ((), ())), preferred_element_type=jnp.float32
        ) * size ** (-0.5)
        scores = scores + own[:, row : row + 1] - cum[row : row + 1, :]
        scores = jnp.where(keep, scores, NEG)
        weights = jnp.exp(scores - jnp.max(scores, axis=-1, keepdims=True))
        denom = jnp.sum(weights, axis=-1, keepdims=True)
        accum = jnp.dot(weights.astype(jnp.bfloat16), values, preferred_element_type=jnp.float32)
        return accum / denom

    attended = head(q_l[...], k_l, v_l, per, size_l)
    mean = jnp.mean(attended * attended, axis=-1, keepdims=True)
    out_l[...] = (attended * lax.rsqrt(mean + EPS)).astype(jnp.bfloat16)
    q = q_s[...]
    lane = lax.broadcasted_iota(jnp.int32, q.shape, 1)
    normed = jnp.zeros(q.shape, jnp.float32)
    for h in range(per):
        mine = (lane >= h * size_s) & (lane < (h + 1) * size_s)
        attended = head(jnp.where(mine, q, jnp.zeros_like(q)), k_s, v_s, h, size_s)
        attended = jnp.where(mine, attended, 0.0)
        mean = jnp.sum(attended * attended, axis=-1, keepdims=True) / size_s
        normed = normed + attended * lax.rsqrt(mean + EPS)
    out_s[...] = normed.astype(jnp.bfloat16)


def attention(cum, steps, per, q_s, k_s, v_s, q_l, k_l, v_l):
    n, rows = k_s.shape[0], q_s.shape[0]
    wide_s, wide_l = q_s.shape[1] // steps, q_l.shape[1] // steps
    of_q = lambda wide: pl.BlockSpec((rows, wide), lambda s: (0, s))
    of_k = lambda wide: pl.BlockSpec((n, k_s.shape[1], wide), lambda s: (0, 0, s))
    return pl.pallas_call(
        functools.partial(attention_kernel, rows, per, wide_s // per, wide_l),
        grid=(steps,),
        in_specs=[pl.BlockSpec((8, cum.shape[1]), lambda s: (s, 0))]
        + [of_q(wide_s), of_k(wide_s), of_k(wide_s), of_q(wide_l), of_k(wide_l), of_k(wide_l)],
        out_specs=[of_q(wide_s), of_q(wide_l)],
        out_shape=[
            jax.ShapeDtypeStruct(q_s.shape, jnp.bfloat16),
            jax.ShapeDtypeStruct(q_l.shape, jnp.bfloat16),
        ],
    )(cum, q_s, k_s, v_s, q_l, k_l, v_l)


def down_kernel(hidden, block, out):
    out[...] = jnp.dot(hidden[...], block[0], preferred_element_type=jnp.float32).astype(out.dtype)


def down_product(hidden, blocks):
    n, depth, wide = blocks.shape
    rows = hidden.shape[0]
    if wide % 128:
        full = jnp.einsum("th,nhc->tnc", hidden, blocks, preferred_element_type=jnp.float32)
        return full.astype(jnp.bfloat16).reshape(rows, -1)
    return pl.pallas_call(
        down_kernel,
        grid=(n,),
        in_specs=[
            pl.BlockSpec((rows, depth), lambda i: (0, 0)),
            pl.BlockSpec((1, depth, wide), lambda i: (i, 0, 0)),
        ],
        out_specs=pl.BlockSpec((rows, wide), lambda i: (0, i)),
        out_shape=jax.ShapeDtypeStruct((rows, n * wide), jnp.bfloat16),
    )(hidden, blocks)


def body(
    residual,
    q_small,
    k_small,
    v_small,
    q_large,
    k_large,
    v_large,
    forget_small,
    forget_large,
    w_out_small,
    w_out_large,
    norm_gain,
    w_gate,
    w_up,
    conv_gate,
    conv_up,
    w_down,
):
    steps = forget_large.shape[1]
    per = forget_small.shape[1] // steps
    rows = q_small.shape[0]
    local_small = jnp.cumsum(jax.nn.log_sigmoid(forget_small), axis=0)
    local_large = jnp.cumsum(jax.nn.log_sigmoid(forget_large), axis=0)
    local = jnp.concatenate(
        [
            local_small.T.reshape(steps, per, rows),
            local_large.T.reshape(steps, 1, rows),
            jnp.zeros((steps, 7 - per, rows), jnp.float32),
        ],
        axis=1,
    ).reshape(steps * 8, rows)
    every, keys_s, values_s, keys_l, values_l, gate_full, up_full, down_blocks = gather_all(
        [local, k_small, v_small, k_large, v_large, w_gate, w_up, w_down],
        [False, True, True, True, False, False, False, False],
    )
    flat = lambda x: x.reshape(-1, x.shape[-1])
    gate_full, up_full = flat(gate_full), flat(up_full)
    totals = every[:, :, -1]
    before = jnp.cumsum(totals, axis=0) - totals
    cum = (every + before[:, :, None]).transpose(1, 0, 2).reshape(steps * 8, -1)
    normed_small, normed_large = attention(
        cum, steps, per, q_small, keys_s, values_s, q_large, keys_l, values_l
    )
    first_part = jnp.dot(normed_small, w_out_small, preferred_element_type=jnp.float32)
    projected = lax.psum_scatter(
        (
            first_part + jnp.dot(normed_large, w_out_large, preferred_element_type=jnp.float32)
        ).astype(jnp.bfloat16),
        "tp",
        scatter_dimension=0,
        tiled=True,
    ).astype(jnp.float32)
    first = residual.astype(jnp.float32) + projected
    normal = (
        first * lax.rsqrt(jnp.mean(first * first, axis=-1, keepdims=True) + EPS) * norm_gain
    ).astype(jnp.bfloat16)
    piece = lax.all_gather(normal, "tp", axis=0, tiled=True)
    gate_part = jnp.dot(piece, gate_full, preferred_element_type=jnp.float32).astype(jnp.bfloat16)
    up_part = jnp.dot(piece, up_full, preferred_element_type=jnp.float32).astype(jnp.bfloat16)
    both = jnp.concatenate([gate_part, up_part], axis=1)
    width = both.shape[0]
    rim = from_behind(both[width - 2 :], "sp", 1)
    extended = jnp.concatenate([rim, both], axis=0).astype(jnp.float32)
    taps = jnp.concatenate([conv_gate, conv_up], axis=1)
    conv = (
        taps[0] * extended[0:width]
        + taps[1] * extended[1 : width + 1]
        + taps[2] * extended[2 : width + 2]
    )
    half = gate_full.shape[1]
    hidden = (jax.nn.silu(conv[:, :half]) * conv[:, half:]).astype(jnp.bfloat16)
    mixed = first + lax.psum_scatter(
        down_product(hidden, down_blocks),
        "tp",
        scatter_dimension=0,
        tiled=True,
    ).astype(jnp.float32)
    return mixed.astype(jnp.bfloat16)


def solution(mesh):
    placed = (
        P(("sp", "tp"), None),
        P("sp", "tp"),
        P("sp", "tp"),
        P("sp", "tp"),
        P("sp", "tp"),
        P("sp", "tp"),
        P("sp", "tp"),
        P("sp", "tp"),
        P("sp", "tp"),
        P("tp", None),
        P("tp", None),
        P(),
        P("sp", "tp"),
        P("sp", "tp"),
        P(None, "tp"),
        P(None, "tp"),
        P("tp", "sp"),
    )
    return jax.shard_map(
        body, mesh=mesh, in_specs=placed, out_specs=P(("sp", "tp"), None), check_vma=False
    )
```

time: 473 us -> 298 us (0.63)
  waiting for transfers between devices: 329 us -> 33.9 us
  Pallas kernels: 0 us -> 219 us
  blocking collectives: 60.3 us -> 8.67 us
  matrix products: 32.2 us -> 8.92 us
  local copies, waits for them, and re-layouts: 22.4 us -> 0.65 us
    all_gather x7 -> x0, waiting for transfers between devices: 300 us -> none  [the longest x1 70.4 us: body(): lax.all_gather(w_gate, 'sp', axis=0, tiled=True)]
    pallas_call x0 -> x3, Pallas kernels: none -> 219 us  [the longest x1 195 us: gather_all(): pl.pallas_call(functools.partial(gather_kernel, n, count, items), out_sha...]
    all_gather x2 -> x0, blocking collectives: 51.6 us -> none  [the longest x1 27.1 us: body(): lax.all_gather(local_large, 'sp', axis=0, tiled=True)]
    dot_general x5 -> x0, matrix products: 21.1 us -> none  [the longest x2 7.76 us: attend(): jnp.einsum('qhk,khd->qhd', weights.astype(jnp.bfloat16), values, preferre...]
    all_gather x3 -> x0, local copies, waits for them, and re-layouts: 12 us -> none  [the longest x1 4.02 us: body(): values_l = lax.all_gather(v_large, 'sp', axis=0, tiled=True)]
    unnamed x31 -> x21, local copies, waits for them, and re-layouts: 7.27 us -> 0.18 us
    reduce_scatter x1, waiting for transfers between devices: 13 us -> 17.7 us  [body(): lax.psum_scatter(down_product(hidden, down_blocks), 'tp', scatter_dimensi...]
  transfers between devices with their start and end apart: 10 -> 3, of which waited for: 9 -> 3; matrix products, arithmetic and copies ran while one was open for 9% -> 0% of each run, Pallas kernels for 0% -> 0%
where the time goes in v2:
time: 298 us
  Pallas kernels  219 us (73%)
  waiting for transfers between devices  33.9 us (11%)
  between operations  13.6 us (5%)
  other arithmetic  11.9 us (4%)
  matrix products  8.92 us (3%)
  blocking collectives  8.67 us (3%)
    pallas_call x1, Pallas kernels, gather_all(): pl.pallas_call(functools.partial(gather_kernel, n, count, items), out_sha...  195 us
    reduce_scatter x1, waiting for transfers between devices, body(): lax.psum_scatter(down_product(hidden, down_blocks), 'tp', scatter_dimensi...  17.7 us
    reduce_scatter x1, waiting for transfers between devices, body(): lax.psum_scatter((first_part + jnp.dot(normed_large, w_out_large, preferr...  15.3 us
    pallas_call x1, Pallas kernels, down_product(): pl.pallas_call(down_kernel, grid=(n,), in_specs=[pl.BlockSpec((rows, dept...  12.5 us
    pallas_call x1, Pallas kernels, attention(): pl.pallas_call(functools.partial(attention_kernel, rows, per, wide_s // p...  10.9 us
    all_gather x1, blocking collectives, body(): piece = lax.all_gather(normal, 'tp', axis=0, tiled=True)  8.67 us
  transfers between devices with their start and end apart: 3, of which 3 were waited for; matrix products, arithmetic and copies ran while one was open for 0% of the time, Pallas kernels for 0%

profile of v2, /device:TPU:0, one launch (start us, length us, event | category | flops | bytes accessed | tf_op | source)
XLA Modules:
  0.0 297.5 jit_solution(7009466427471700374)
XLA Ops:
  6.5 0.0 copy-start
  6.5 0.0 reduce-scatter.3.cloned.1.call-start
  6.5 0.8 fusion.5
  7.4 0.1 copy.23
  7.5 0.2 reduce_window_sum.33
  7.7 0.7 fusion.6
  8.4 0.1 copy.25
  8.6 0.2 reduce_window_sum.34
  8.7 0.1 copy.26
  8.8 0.1 pad.7.clone
  8.9 0.7 maximum_bitcast_fusion.refs_0_
  9.6 195.1 %shard_map.163 = (f32[16,32,128]{2,1,0:T(8,128)}, bf16[16,128,512]{2,1,0:T(8,128)(2,1)}, bf16[16,128,512]{2,1,0:T(8,128)(2,1)}, bf16[16,128,512]{2,1,0:T(8,128)(...) custom-call(f32[32,128]{1,0:T(8,128)} %maximum_bitcast_fusion.refs_0, ...), custom_call_target="tpu_custom_call" | custom-call | tf_op jit(solution)/shard_map/pallas_call | solution.py:169
  204.7 1.5 fusion.8
  206.2 1.8 copy_bitcast_fusion.cum
  208.0 10.9 %shard_map.164 = (bf16[128,512]{1,0:T(8,128)(2,1)}, bf16[128,512]{1,0:T(8,128)(2,1)}) custom-call(f32[32,2048]{1,0:T(8,128)} %copy_bitcast_fusion.cum, bf16[128,512]{1,0:T(8,128)(2,1)} %q_s.1, bf16[16,128,512]{2,1,0:T(8,128)(2,1)} %get-tuple-element.16.k_s, bf16[16,128,512]{2,1,0:T(8,128)(2,1)} %get-tuple-element.17.v_s, bf16[128,512]{1,0:T(8,128)(2,1)} %q_l.1, ...), custom_call_target="tpu_custom_call" | custom-call | tf_op jit(solution)/shard_map/pallas_call | solution.py:228
  218.9 0.0 copy-start.3
  218.9 0.0 copy-start.4
  218.9 0.0 copy-done
  218.9 1.5 fusion.9
  220.4 0.1 copy-done.3
  220.6 0.0 copy-done.4
  220.6 0.0 copy-start.5
  220.6 0.0 copy-start.6
  220.6 0.0 copy-start.1
  220.6 0.0 copy-start.7
  220.6 1.3 fusion
  221.9 0.0 reduce-scatter.3.cloned.1.call-update
  221.9 0.0 reduce-scatter.5.cloned.1.call-start
  222.0 0.0 copy-done.5
  222.0 0.0 copy-done.6
  222.0 15.3 %reduce-scatter.3.cloned.1.call-done = bf16[64,2048]{1,0:T(8,128)(2,1)} async-done(((bf16[128,2048]{1,0:T(8,128)(2,1)}), bf16[64,2048]{1,0:T(8,128)(2,1)}) %reduce-scatter.3.cloned.1.call-update) | async-done | bytes 262160 | tf_op jit(solution)/shard_map/reduce_scatter | solution.py:308
  237.4 0.0 copy-done.1
  237.4 1.1 multiply_reduce_fusion
  238.5 0.0 copy-done.7
  238.5 1.1 multiply_convert_fusion
  239.6 0.0 slice-start
  239.6 8.7 %all_gather.3 = bf16[128,2048]{1,0:T(8,128)(2,1)S(1)} all-gather(bf16[64,2048]{1,0:T(8,128)(2,1)S(1)} %multiply_convert_fusion), channel_id=1, replica_groups=mesh['sp'=16,'tp'=2] {'tp'}, dimensions={0}, use_global_device_ids=true | all-gather | bytes 786432 | tf_op jit(solution)/shard_map/all_gather | solution.py:320
  248.3 0.0 slice-start.1
  248.3 4.8 %convolution_convert_fusion.1 = bf16[128,2048]{1,0:T(8,128)(2,1)S(1)} fusion(bf16[128,2048]{1,0:T(8,128)(2,1)S(1)} %all_gather.3, bf16[2048,2048]{1,0:T(8,128)(2,1)} %bitcast.29), kind=kOutput, calls=%fused_computation.2 | convolution fusion | flops 1074003968 | bytes 9437184 | tf_op jit(solution)/shard_map/dot_general | solution.py:321
  253.1 0.0 slice-done
  253.1 0.0 slice-done.1
  253.1 1.3 convolution_convert_fusion
  254.5 1.3 collective-permute-start
  255.8 0.8 collective-permute-done
  256.6 0.3 maximum_convert_fusion
  256.9 0.6 fusion.1
  257.5 1.1 fusion.3.hidden
  258.7 0.0 copy-start.2
  258.7 12.5 %shard_map.165 = bf16[128,2048]{1,0:T(8,128)(2,1)} custom-call(bf16[128,2048]{1,0:T(8,128)(2,1)} %fusion.3.hidden, bf16[16,2048,128]{2,1,0:T(8,128)(2,1)} %get-tuple-element.24.block), custom_call_target="tpu_custom_call" | custom-call | tf_op jit(solution)/shard_map/pallas_call | solution.py:251
  271.2 0.0 reduce-scatter.5.cloned.1.call-update
  271.2 17.7 %reduce-scatter.5.cloned.1.call-done = bf16[64,2048]{1,0:T(8,128)(2,1)} async-done(((bf16[128,2048]{1,0:T(8,128)(2,1)}), bf16[64,2048]{1,0:T(8,128)(2,1)}) %reduce-scatter.5.cloned.1.call-update) | async-done | bytes 262160 | tf_op jit(solution)/shard_map/reduce_scatter | solution.py:335
  288.9 0.0 copy-done.2
  288.9 1.7 add_convert_fusion
  (8 shorter events, 0.1 us)
Async XLA Ops:
  6.5 212.4 %copy-start = (bf16[512,2048]{1,0:T(8,128)(2,1)S(1)}, bf16[512,2048]{1,0:T(8,128)(2,1)}, u32[]{:S(2)}) copy-start(bf16[512,2048]{1,0:T(8,128)(2,1)} %param.26) | copy-start | bytes 6291460
  6.5 230.8 %reduce-scatter.3.cloned.1.call-start = ((), (), s32[]{:S(2)}) async-start(), calls=%async_computation.2 | async-start | bytes 786432 | tf_op jit(solution)/shard_map/reduce_scatter | solution.py:308
  218.9 1.7 copy-start.3
  218.9 1.7 copy-start.4
  220.6 1.4 copy-start.5
  220.6 1.4 copy-start.6
  220.6 16.8 %copy-start.1 = (bf16[64,2048]{1,0:T(8,128)(2,1)S(1)}, bf16[64,2048]{1,0:T(8,128)(2,1)}, u32[]{:S(2)}) copy-start(bf16[64,2048]{1,0:T(8,128)(2,1)} %param.17) | copy-start | bytes 786436
  220.6 17.9 %copy-start.7 = (f32[2048]{0:T(1024)S(1)}, f32[2048]{0:T(1024)}, u32[]{:S(2)}) copy-start(f32[2048]{0:T(1024)} %param.28) | copy-start | bytes 24580
  221.9 67.0 %reduce-scatter.5.cloned.1.call-start = ((), (), s32[]{:S(2)}) async-start(), calls=%async_computation.3 | async-start | bytes 786432 | tf_op jit(solution)/shard_map/reduce_scatter | solution.py:335
  239.6 13.5 %slice-start = ((s8[8388608]{0:T(1024)(128)(4,1)}), s8[4194304]{0:T(1024)(128)(4,1)S(1)}, s32[]{:S(2)}) async-start(s8[8388608]{0:T(1024)(128)(4,1)} %bitcast.26), calls=%async_computation.4 | async-start | bytes 8388608
  248.3 4.8 %slice-start.1 = ((s8[8388608]{0:T(1024)(128)(4,1)}), s8[4194304]{0:T(1024)(128)(4,1)S(1)}, s32[]{:S(2)}) async-start(s8[8388608]{0:T(1024)(128)(4,1)} %bitcast.26), calls=%async_computation.5 | async-start | bytes 8388608
  254.5 2.1 collective-permute-start
  258.7 30.3 %copy-start.2 = (bf16[64,2048]{1,0:T(8,128)(2,1)S(1)}, bf16[64,2048]{1,0:T(8,128)(2,1)}, u32[]{:S(2)}) copy-start(bf16[64,2048]{1,0:T(8,128)(2,1)} %reduce-scatter.3.cloned.1.call-done) | copy-start | bytes 786436
Sparse Core Ops, SparseCore 0:
  222.1 15.2 reduce-scatter.2
  271.3 17.5 reduce-scatter.4

commit v3 on v2

--- a/solution.py
+++ b/solution.py
@@ -18,7 +18,7 @@
 
 
 PLANE = 4
-PIECE = 1 << 18
+PIECE = 1 << 17
 UP, DOWN, UP_OTHER, DOWN_OTHER, ACROSS, CORE, CORE_OTHER = range(7)
 OWN, OTHER = 0, 1
 MESH = pl.DeviceIdType.MESH
@@ -238,8 +238,70 @@
     )(cum, q_s, k_s, v_s, q_l, k_l, v_l)
 
 
-def down_kernel(hidden, block, out):
-    out[...] = jnp.dot(hidden[...], block[0], preferred_element_type=jnp.float32).astype(out.dtype)
+def exchange_kernel(n, spread, x, out, local_sem, send_sem, recv_sem):
+    me = lax.axis_index("tp")
+    barrier = pltpu.get_barrier_semaphore()
+    for d in range(1, n):
+        pl.semaphore_signal(barrier, inc=1, device_id={"tp": lax.rem(me + d, n)}, device_id_type=MESH)
+    pl.semaphore_wait(barrier, n - 1)
+    copies = []
+    for d in range(1, n):
+        target = lax.rem(me + d, n)
+        copy = pltpu.make_async_remote_copy(
+            src_ref=x.at[target] if spread else x,
+            dst_ref=out.at[me],
+            send_sem=send_sem.at[d],
+            recv_sem=recv_sem.at[d],
+            device_id={"tp": target},
+            device_id_type=MESH,
+        )
+        copy.start()
+        copies.append(copy)
+    local = pltpu.make_async_copy(x.at[me] if spread else x, out.at[me], local_sem)
+    local.start()
+    for d in range(1, n):
+        view = out.at[lax.rem(me - d + n, n)]
+        pltpu.make_async_remote_copy(
+            src_ref=view,
+            dst_ref=view,
+            send_sem=send_sem.at[d],
+            recv_sem=recv_sem.at[d],
+            device_id={"tp": lax.rem(me + d, n)},
+            device_id_type=MESH,
+        ).wait_recv()
+    for copy in copies:
+        copy.wait_send()
+    local.wait()
+
+
+def exchange(x, spread, number):
+    n = lax.axis_size("tp")
+    block = x.shape[1:] if spread else x.shape
+    if n == 1:
+        return x if spread else x[None]
+    return pl.pallas_call(
+        functools.partial(exchange_kernel, n, spread),
+        out_shape=jax.ShapeDtypeStruct((n,) + block, x.dtype),
+        in_specs=[pl.BlockSpec(memory_space=pltpu.VMEM)],
+        out_specs=pl.BlockSpec(memory_space=pltpu.VMEM),
+        scratch_shapes=[
+            pltpu.SemaphoreType.DMA,
+            pltpu.SemaphoreType.DMA((n,)),
+            pltpu.SemaphoreType.DMA((n,)),
+        ],
+        compiler_params=pltpu.CompilerParams(collective_id=number, has_side_effects=True),
+    )(x)
+
+
+def sum_over_tp(part, number):
+    n = lax.axis_size("tp")
+    parts = exchange(part.astype(jnp.bfloat16).reshape(n, -1, part.shape[-1]), True, number)
+    return jnp.sum(parts.astype(jnp.float32), axis=0)
+
+
+def down_kernel(hidden, blocks, out):
+    wide = jnp.concatenate([blocks[i] for i in range(blocks.shape[0])], axis=1)
+    out[...] = jnp.dot(hidden[...], wide, preferred_element_type=jnp.float32).astype(out.dtype)
 
 
 def down_product(hidden, blocks):
@@ -248,14 +310,15 @@
     if wide % 128:
         full = jnp.einsum("th,nhc->tnc", hidden, blocks, preferred_element_type=jnp.float32)
         return full.astype(jnp.bfloat16).reshape(rows, -1)
+    fan = 4 if n % 4 == 0 else 1
     return pl.pallas_call(
         down_kernel,
-        grid=(n,),
+        grid=(n // fan,),
         in_specs=[
             pl.BlockSpec((rows, depth), lambda i: (0, 0)),
-            pl.BlockSpec((1, depth, wide), lambda i: (i, 0, 0)),
+            pl.BlockSpec((fan, depth, wide), lambda i: (i, 0, 0)),
         ],
-        out_specs=pl.BlockSpec((rows, wide), lambda i: (0, i)),
+        out_specs=pl.BlockSpec((rows, fan * wide), lambda i: (0, i)),
         out_shape=jax.ShapeDtypeStruct((rows, n * wide), jnp.bfloat16),
     )(hidden, blocks)
 
@@ -305,19 +368,14 @@
         cum, steps, per, q_small, keys_s, values_s, q_large, keys_l, values_l
     )
     first_part = jnp.dot(normed_small, w_out_small, preferred_element_type=jnp.float32)
-    projected = lax.psum_scatter(
-        (
-            first_part + jnp.dot(normed_large, w_out_large, preferred_element_type=jnp.float32)
-        ).astype(jnp.bfloat16),
-        "tp",
-        scatter_dimension=0,
-        tiled=True,
-    ).astype(jnp.float32)
+    projected = sum_over_tp(
+        first_part + jnp.dot(normed_large, w_out_large, preferred_element_type=jnp.float32), 1
+    )
     first = residual.astype(jnp.float32) + projected
     normal = (
         first * lax.rsqrt(jnp.mean(first * first, axis=-1, keepdims=True) + EPS) * norm_gain
     ).astype(jnp.bfloat16)
-    piece = lax.all_gather(normal, "tp", axis=0, tiled=True)
+    piece = flat(exchange(normal, False, 2))
     gate_part = jnp.dot(piece, gate_full, preferred_element_type=jnp.float32).astype(jnp.bfloat16)
     up_part = jnp.dot(piece, up_full, preferred_element_type=jnp.float32).astype(jnp.bfloat16)
     both = jnp.concatenate([gate_part, up_part], axis=1)
@@ -332,12 +390,7 @@
     )
     half = gate_full.shape[1]
     hidden = (jax.nn.silu(conv[:, :half]) * conv[:, half:]).astype(jnp.bfloat16)
-    mixed = first + lax.psum_scatter(
-        down_product(hidden, down_blocks),
-        "tp",
-        scatter_dimension=0,
-        tiled=True,
-    ).astype(jnp.float32)
+    mixed = first + sum_over_tp(down_product(hidden, down_blocks), 3)
     return mixed.astype(jnp.bfloat16)
 
 

time: 298 us -> 281 us (0.943)
  Pallas kernels: 219 us -> 253 us
  waiting for transfers between devices: 33.9 us -> 0.72 us
  between operations: 13.6 us -> 0.21 us
  blocking collectives: 8.67 us -> 0 us
  matrix products: 8.92 us -> 12.3 us
    reduce_scatter x2 -> x0, waiting for transfers between devices: 33.1 us -> none  [the longest x1 17.7 us: body(): lax.psum_scatter(down_product(hidden, down_blocks), 'tp', scatter_dimensi...]
    pallas_call x1 -> x4, Pallas kernels: 12.5 us -> 37.7 us  [the longest x3 31.9 us: exchange(): pl.pallas_call(functools.partial(exchange_kernel, n, spread), out_shape=j...]
    pallas_call x1, Pallas kernels: 195 us -> 204 us  [gather_all(): pl.pallas_call(functools.partial(gather_kernel, n, count, items), out_sha...]
    all_gather x1 -> x0, blocking collectives: 8.67 us -> none  [body(): piece = lax.all_gather(normal, 'tp', axis=0, tiled=True)]
    dot_general x1, matrix products: 1.3 us -> 4.68 us  [body(): jnp.dot(piece, up_full, preferred_element_type=jnp.float32)]
  transfers between devices with their start and end apart: 3 -> 1, of which waited for: 3 -> 1; matrix products, arithmetic and copies ran while one was open for 0% -> 0% of each run, Pallas kernels for 0% -> 0%
where the time goes in v3:
time: 281 us; the launch traced here: 280 us
  Pallas kernels  253 us (90%)
  matrix products  12.3 us (4%)
  other arithmetic  12 us (4%)
    pallas_call x1, Pallas kernels, gather_all(): pl.pallas_call(functools.partial(gather_kernel, n, count, items), out_sha...  204 us
    pallas_call x3, Pallas kernels, exchange(): pl.pallas_call(functools.partial(exchange_kernel, n, spread), out_shape=j...  31.9 us
    pallas_call x1, Pallas kernels, attention(): pl.pallas_call(functools.partial(attention_kernel, rows, per, wide_s // p...  10.9 us
    pallas_call x1, Pallas kernels, down_product(): pl.pallas_call(down_kernel, grid=(n // fan,), in_specs=[pl.BlockSpec((row...  5.75 us
  transfers between devices with their start and end apart: 1, of which 1 were waited for; matrix products, arithmetic and copies ran while one was open for 0% of the time, Pallas kernels for 0%

profile of v3, /device:TPU:0, one launch (start us, length us, event | category | flops | bytes accessed | tf_op | source)
XLA Modules:
  0.0 280.2 jit_solution(1954177974084928106)
XLA Ops:
  0.0 0.0 copy-start
  0.0 0.8 fusion.5
  0.9 0.1 copy.23
  1.0 0.2 reduce_window_sum.33
  1.2 0.7 fusion.6
  1.9 0.1 copy.25
  2.0 0.2 reduce_window_sum.34
  2.2 0.1 copy.26
  2.3 0.1 pad.7.clone
  2.3 0.7 maximum_bitcast_fusion.refs_0_
  3.0 204.4 %shard_map.163 = (f32[16,32,128]{2,1,0:T(8,128)}, bf16[16,128,512]{2,1,0:T(8,128)(2,1)}, bf16[16,128,512]{2,1,0:T(8,128)(2,1)}, bf16[16,128,512]{2,1,0:T(8,128)(...) custom-call(f32[32,128]{1,0:T(8,128)} %maximum_bitcast_fusion.refs_0, ...), custom_call_target="tpu_custom_call" | custom-call | tf_op jit(solution)/shard_map/pallas_call | solution.py:169
  207.4 1.4 fusion.8
  208.9 1.8 copy_bitcast_fusion.cum
  210.7 10.9 %shard_map.164 = (bf16[128,512]{1,0:T(8,128)(2,1)}, bf16[128,512]{1,0:T(8,128)(2,1)}) custom-call(f32[32,2048]{1,0:T(8,128)} %copy_bitcast_fusion.cum, bf16[128,512]{1,0:T(8,128)(2,1)} %q_s.1, bf16[16,128,512]{2,1,0:T(8,128)(2,1)} %get-tuple-element.16.k_s, bf16[16,128,512]{2,1,0:T(8,128)(2,1)} %get-tuple-element.17.v_s, bf16[128,512]{1,0:T(8,128)(2,1)} %q_l.1, ...), custom_call_target="tpu_custom_call" | custom-call | tf_op jit(solution)/shard_map/pallas_call | solution.py:228
  221.6 0.0 copy-start.3
  221.6 0.0 copy-start.4
  221.6 0.0 copy-done
  221.6 1.5 fusion.9
  223.1 0.1 copy-done.3
  223.2 0.0 copy-done.4
  223.2 0.0 copy-start.2
  223.2 1.3 fusion
  224.5 0.0 copy-start.7
  224.5 11.1 %shard_map.165 = bf16[2,64,2048]{2,1,0:T(8,128)(2,1)} custom-call(bf16[2,64,2048]{2,1,0:T(8,128)(2,1)} %bitcast.34), custom_call_target="tpu_custom_call" | custom-call | tf_op jit(solution)/shard_map/pallas_call | solution.py:282
  235.6 1.2 convert_reduce_fusion.1
  236.8 0.0 copy-done.2
  236.8 0.2 multiply_reduce_fusion
  237.0 0.0 copy-done.7
  237.0 0.8 multiply_convert_fusion.x
  237.8 10.1 %shard_map.166 = bf16[2,64,2048]{2,1,0:T(8,128)(2,1)} custom-call(bf16[64,2048]{1,0:T(8,128)(2,1)} %multiply_convert_fusion.x), custom_call_target="tpu_custom_call" | custom-call | tf_op jit(solution)/shard_map/pallas_call | solution.py:282
  247.9 0.0 copy-start.1
  247.9 4.9 %convolution_convert_fusion.1 = bf16[128,2048]{1,0:T(8,128)(2,1)S(1)} fusion(bf16[128,2048]{1,0:T(8,128)(2,1)} %bitcast.31, bf16[2048,2048]{1,0:T(8,128)(2,1)} %bitcast.30), kind=kOutput, calls=%fused_computation.2 | convolution fusion | flops 1074003968 | bytes 9437184 | tf_op jit(solution)/shard_map/dot_general | solution.py:379
  252.8 0.0 copy-done.1
  252.8 0.0 copy-start.5
  252.8 0.0 copy-start.6
  252.8 4.7 %convolution_convert_fusion = bf16[128,2048]{1,0:T(8,128)(2,1)S(1)} fusion(bf16[128,2048]{1,0:T(8,128)(2,1)S(1)} %bitcast.32, bf16[2048,2048]{1,0:T(8,128)(2,1)} %bitcast.29), kind=kOutput, calls=%fused_computation.1 | convolution fusion | flops 1074003968 | bytes 9437184 | tf_op jit(solution)/shard_map/dot_general | solution.py:380
  257.6 1.3 collective-permute-start
  258.9 0.0 copy-done.5
  258.9 0.0 copy-done.6
  259.0 0.7 collective-permute-done
  259.7 0.3 maximum_convert_fusion
  260.0 0.6 fusion.1
  260.6 1.2 fusion.3.hidden
  261.8 5.7 %shard_map.167 = bf16[128,2048]{1,0:T(8,128)(2,1)} custom-call(bf16[128,2048]{1,0:T(8,128)(2,1)} %fusion.3.hidden, bf16[16,2048,128]{2,1,0:T(8,128)(2,1)} %get-tuple-element.24.blocks), custom_call_target="tpu_custom_call" | custom-call | tf_op jit(solution)/shard_map/pallas_call | solution.py:314
  267.5 10.8 %shard_map.168 = bf16[2,64,2048]{2,1,0:T(8,128)(2,1)} custom-call(bf16[2,64,2048]{2,1,0:T(8,128)(2,1)} %bitcast.33), custom_call_target="tpu_custom_call" | custom-call | tf_op jit(solution)/shard_map/pallas_call | solution.py:282
  278.3 1.2 convert_reduce_fusion
  279.4 0.8 add_convert_fusion
  (7 shorter events, 0.1 us)
Async XLA Ops:
  0.0 221.6 %copy-start = (bf16[512,2048]{1,0:T(8,128)(2,1)S(1)}, bf16[512,2048]{1,0:T(8,128)(2,1)}, u32[]{:S(2)}) copy-start(bf16[512,2048]{1,0:T(8,128)(2,1)} %param.26) | copy-start | bytes 6291460
  221.6 1.7 copy-start.3
  221.6 1.7 copy-start.4
  223.2 13.6 %copy-start.2 = (bf16[64,2048]{1,0:T(8,128)(2,1)S(1)}, bf16[64,2048]{1,0:T(8,128)(2,1)}, u32[]{:S(2)}) copy-start(bf16[64,2048]{1,0:T(8,128)(2,1)} %param.17) | copy-start | bytes 786436
  224.5 12.5 %copy-start.7 = (f32[2048]{0:T(1024)S(1)}, f32[2048]{0:T(1024)}, u32[]{:S(2)}) copy-start(f32[2048]{0:T(1024)} %param.28) | copy-start | bytes 24580
  247.9 4.9 %copy-start.1 = (bf16[2,64,2048]{2,1,0:T(8,128)(2,1)S(1)}, bf16[2,64,2048]{2,1,0:T(8,128)(2,1)}, u32[]{:S(2)}) copy-start(bf16[2,64,2048]{2,1,0:T(8,128)(2,1)} %shard_map.166) | copy-start | bytes 1572868
  252.8 6.0 %copy-start.5 = (f32[3,2048]{1,0:T(4,128)S(1)}, f32[3,2048]{1,0:T(4,128)}, u32[]{:S(2)}) copy-start(f32[3,2048]{1,0:T(4,128)} %param.31) | copy-start | bytes 73732
  252.8 6.1 %copy-start.6 = (f32[3,2048]{1,0:T(4,128)S(1)}, f32[3,2048]{1,0:T(4,128)}, u32[]{:S(2)}) copy-start(f32[3,2048]{1,0:T(4,128)} %param.32) | copy-start | bytes 73732
  257.6 2.1 collective-permute-start
